TPU v7x, 32 devices: a whole 2x2x4 slice. The times are simulated.
32 devices in a mesh: sp: 8 (over z, core), tp: 4 (over y, x).
Axes of the slice: x: 2, y: 2, z: 4, core: 2. Of those that a mesh axis runs over, the one named last changes fastest.
Arguments:
- moe_input: bfloat16 [1024, 2048], P('sp', 'tp'), may hold values from -6 to 6
- cotangent: bfloat16 [1024, 2048], P('sp', 'tp'), may hold values from -6 to 6
- routes: int32 [1024, 2], P('sp'), may hold values from 0 to 7, all different within a row; in each aligned block of 128 rows (0 to 127, 128 to 255, ...) at most 64 rows name the same one
- route_weight: float32 [1024, 2], P('sp'), may hold values from 0.1 to 1
- w_gate: bfloat16 [8, 2816, 2048], P('sp', 'tp'), may hold values from -0.125 to 0.125
- w_up: bfloat16 [8, 2816, 2048], P('sp', 'tp'), may hold values from -0.125 to 0.125
- w_down: bfloat16 [8, 2816, 2048], P('sp', 'tp'), may hold values from -0.109375 to 0.109375
- v_value: bfloat16 [1024, 1024], P('sp', 'tp'), may hold values from -6 to 6
- v_gate: bfloat16 [1024, 1024], P('sp', 'tp'), may hold values from -12 to 12
- conv_out: bfloat16 [1024, 1024], P('sp', 'tp'), may hold values from -6 to 6
- row_mean: float32 [1024], P('sp'), may hold values from -3 to 3
- row_rstd: float32 [1024], P('sp'), may hold values from 0.5 to 2
- ln_gain: float32 [1024], P('tp'), may hold values from 0.1 to 1.9
- taps: bfloat16 [31, 1024], P(None, 'tp'), may hold values from -1 to 1
- out_proj: bfloat16 [2048, 1024], P('sp', 'tp'), may hold values from -0.1875 to 0.1875
Outputs:
- gate_grad: bfloat16 [8, 2816, 2048], P('sp', 'tp')
- up_grad: bfloat16 [8, 2816, 2048], P('sp', 'tp')
- down_grad: bfloat16 [8, 2816, 2048], P('sp', 'tp')
- proj_grad: float32 [2048, 1024], P('sp', 'tp')
- stream_grad: bfloat16 [1024, 2048], P('sp', 'tp')
- value_grad: bfloat16 [1024, 1024], P('sp', 'tp')
- gating_grad: bfloat16 [1024, 1024], P('sp', 'tp')
Inputs may be any that keep to these rules, and one draw needn't show every extreme that they name: `routes`: in the rows of one device no expert is named more than 64 times.
All inputs are finite; a program needn't handle non-finite values.
Results may differ from a plain program's by a relative error of at most 0.025.
Values may be sent and summed in bfloat16 or wider, within the bound.
A program may use at most 64 MiB of HBM per device.

v0:
```python
import jax
import jax.numpy as jnp
from jax import lax
from jax.sharding import PartitionSpec as P


def passed_along(value, axis, steps):
    count = lax.axis_size(axis)
    leading, last = (max(0, -steps), min(count, count - steps))
    return lax.ppermute(value, axis, [(source, source + steps) for source in range(leading, last)])


def route_targets(routes, experts, capacity):
    flat_routes = routes.reshape(-1)
    member = (flat_routes[:, None] == jnp.arange(experts, dtype=jnp.int32)[None, :]).astype(
        jnp.int32
    )
    earlier = jnp.cumsum(member, axis=0) - member
    slot_index = jnp.sum(earlier * member, axis=1)
    return flat_routes * capacity + slot_index


def contract_rows(left, right):
    return lax.dot_general(
        left, right, (((0,), (0,)), ((), ())), preferred_element_type=jnp.float32
    )


def contract_cols(left, right):
    return lax.dot_general(
        left, right, (((1,), (1,)), ((), ())), preferred_element_type=jnp.float32
    )


def shards(
    moe_input,
    cotangent,
    routes,
    route_weight,
    w_gate,
    w_up,
    w_down,
    v_value,
    v_gate,
    conv_out,
    row_mean,
    row_rstd,
    ln_gain,
    taps,
    out_proj,
):
    experts = lax.axis_size("sp")
    tokens = routes.shape[0]
    capacity = 4 * tokens // experts
    total = experts * capacity
    buffer_row = route_targets(routes, experts, capacity)
    token_index = jnp.arange(2 * tokens, dtype=jnp.int32) // 2
    weights = route_weight.reshape(-1)
    width = moe_input.shape[1]
    picked = moe_input[token_index]
    weighted = (weights[:, None] * cotangent[token_index].astype(jnp.float32)).astype(jnp.bfloat16)
    rows_buf = jnp.zeros((total, width), jnp.bfloat16).at[buffer_row].set(picked)
    cotan_buf = jnp.zeros((total, width), jnp.bfloat16).at[buffer_row].set(weighted)
    rows_buf, cotan_buf = (
        rows_buf.reshape(experts, capacity, width),
        cotan_buf.reshape(experts, capacity, width),
    )
    part_rows, part_cotan = (
        lax.all_to_all(rows_buf, "sp", split_axis=0, concat_axis=0, tiled=True),
        lax.all_to_all(cotan_buf, "sp", split_axis=0, concat_axis=0, tiled=True),
    )
    arrived_rows, arrived_cotan = (
        lax.all_gather(part_rows, "tp", axis=2, tiled=True),
        lax.all_gather(part_cotan, "tp", axis=2, tiled=True),
    )
    width = arrived_rows.shape[2]
    expert_in = arrived_rows.reshape(total, width)
    expert_cot = arrived_cotan.reshape(total, width)
    gate_w = w_gate[0]
    up_w = w_up[0]
    down_w = w_down[0]
    gate_pre = contract_cols(expert_in, gate_w)
    up_pre = contract_cols(expert_in, up_w)
    gate_sig = jax.nn.sigmoid(gate_pre)
    gate_act = gate_pre * gate_sig
    hidden = (gate_act * up_pre).astype(jnp.bfloat16)
    down_g = contract_rows(hidden, expert_cot).astype(jnp.bfloat16)
    hidden_grad = contract_cols(expert_cot, down_w)
    gate_delta = (hidden_grad * up_pre * gate_sig * (1.0 + gate_pre * (1.0 - gate_sig))).astype(
        jnp.bfloat16
    )
    up_delta = (hidden_grad * gate_act).astype(jnp.bfloat16)
    gate_g = contract_rows(gate_delta, expert_in).astype(jnp.bfloat16)
    up_g = contract_rows(up_delta, expert_in).astype(jnp.bfloat16)
    partial_value = jnp.dot(gate_delta, gate_w, preferred_element_type=jnp.float32) + jnp.dot(
        up_delta, up_w, preferred_element_type=jnp.float32
    )
    row_share = lax.psum_scatter(
        partial_value.astype(jnp.bfloat16), "tp", scatter_dimension=1, tiled=True
    )
    slice_width = row_share.shape[1]
    returned = lax.all_to_all(
        row_share.reshape(experts, capacity, slice_width),
        "sp",
        split_axis=0,
        concat_axis=0,
        tiled=True,
    )
    mine = (
        returned.reshape(total, slice_width)[buffer_row]
        .astype(jnp.float32)
        .reshape(tokens, 2, slice_width)
    )
    stream = (cotangent.astype(jnp.float32) + (mine[:, 0] + mine[:, 1])).astype(jnp.bfloat16)
    full_stream = lax.all_gather(stream, "tp", axis=1, tiled=True)
    normed = (conv_out.astype(jnp.float32) - row_mean[:, None]) * row_rstd[:, None]
    scaled_norm = normed * ln_gain[None, :]
    norm_sig = jax.nn.sigmoid(scaled_norm)
    mixed = (scaled_norm * norm_sig).astype(jnp.bfloat16)
    columns = full_stream
    mixed_grad = jnp.dot(
        columns,
        lax.all_gather(out_proj, "sp", axis=0, tiled=True),
        preferred_element_type=jnp.float32,
    )
    columns = full_stream
    proj_g = lax.psum_scatter(
        contract_rows(columns, mixed).astype(jnp.bfloat16), "sp", scatter_dimension=0, tiled=True
    ).astype(jnp.float32)
    channels = out_proj.shape[1] * lax.axis_size("tp")
    norm_grad = mixed_grad * norm_sig * (1.0 + scaled_norm * (1.0 - norm_sig)) * ln_gain[None, :]
    first_sum, second_sum = lax.psum(
        (jnp.sum(norm_grad, axis=1), jnp.sum(norm_grad * normed, axis=1)), "tp"
    )
    first_mean = first_sum[:, None] / channels
    second_mean = second_sum[:, None] / channels
    conv_grad = row_rstd[:, None] * (norm_grad - first_mean - normed * second_mean)
    kernel = taps.shape[0]
    following = passed_along(conv_grad[: kernel - 1], "sp", -1)
    extended = jnp.concatenate([conv_grad, following], axis=0)
    tap_values = taps.astype(jnp.float32)
    unit_grad = jnp.zeros_like(conv_grad)
    for offset in range(kernel):
        lead = kernel - 1 - offset
        unit_grad = unit_grad + tap_values[offset][None, :] * extended[lead : lead + tokens]
    value_sig = jax.nn.sigmoid(v_gate.astype(jnp.float32))
    value_g = (unit_grad * value_sig).astype(jnp.bfloat16)
    gating_g = (unit_grad * v_value.astype(jnp.float32) * value_sig * (1.0 - value_sig)).astype(
        jnp.bfloat16
    )
    return (gate_g[None], up_g[None], down_g[None], proj_g, stream, value_g, gating_g)


def solution(mesh):
    return jax.shard_map(
        shards,
        mesh=mesh,
        in_specs=(
            P("sp", "tp"),
            P("sp", "tp"),
            P("sp", None),
            P("sp", None),
            P("sp", "tp", None),
            P("sp", "tp", None),
            P("sp", "tp", None),
            P("sp", "tp"),
            P("sp", "tp"),
            P("sp", "tp"),
            P("sp"),
            P("sp"),
            P("tp"),
            P(None, "tp"),
            P("sp", "tp"),
        ),
        out_specs=(
            P("sp", "tp", None),
            P("sp", "tp", None),
            P("sp", "tp", None),
            P("sp", "tp"),
            P("sp", "tp"),
            P("sp", "tp"),
            P("sp", "tp"),
        ),
        check_vma=False,
    )
```

profile of v0, /device:TPU:0, one launch (start us, length us, event | category | flops | bytes accessed | tf_op | source)
XLA Modules:
  0.0 229.9 jit_solution(8924655824834304868)
XLA Ops:
  11.2 3.9 %scatter_custom_fusion.1 = bf16[512,512]{1,0:T(8,128)(2,1)S(1)} fusion(s32[256]{0:T(256)S(1)} %bitcast.123, bf16[128,512]{1,0:T(8,128)(2,1)} %param.15, s32[1024]{0:T(1024)S(1)} %pad_clamp_fusion.1, bf16[]{:T(256)} %constant.29.clone.1), kind=kCustom, calls=%fused_computation.94 | custom fusion | bytes 524800 | tf_op jit(solution)/shard_map/scatter | solution.py:62
  15.1 21.6 %all_to_all.15 = bf16[8,64,512]{2,1,0:T(8,128)(2,1)} all-to-all(bf16[8,64,512]{2,1,0:T(8,128)(2,1)S(1)} %bitcast.90), channel_id=1, replica_groups=mesh['sp'=8,'tp'=4] {'sp'}, dimensions={0} | all-to-all | bytes 1048576 | tf_op jit(solution)/shard_map/all_to_all | solution.py:69
  37.1 2.9 %scatter_custom_fusion = bf16[512,512]{1,0:T(8,128)(2,1)S(1)} fusion(s32[256]{0:T(256)S(1)} %bitcast.124, f32[256]{0:T(256)S(1)} %mul.427, bf16[]{:T(256)} %constant.29.clone.1, bf16[128,512]{1,0:T(8,128)(2,1)S(1)} %copy-done.3, s32[1024]{0:T(1024)S(1)} %pad_clamp_fusion.1), kind=kCustom, calls=%fused_computation.89 | custom fusion | flops 393216 | bytes 660482 | tf_op jit(solution)/shard_map/scatter | solution.py:63
  39.9 18.4 %all_to_all.16 = bf16[8,64,512]{2,1,0:T(8,128)(2,1)} all-to-all(bf16[8,64,512]{2,1,0:T(8,128)(2,1)S(1)} %bitcast.89), channel_id=1, replica_groups=mesh['sp'=8,'tp'=4] {'sp'}, dimensions={0} | all-to-all | bytes 1048576 | tf_op jit(solution)/shard_map/all_to_all | solution.py:70
  58.6 12.3 %all-gather.6.cloned.1.call-done = bf16[8,64,2048]{2,1,0:T(8,128)(2,1)} async-done(((bf16[8,64,512]{2,1,0:T(8,128)(2,1)}), bf16[8,64,2048]{2,1,0:T(8,128)(2,1)}) %all-gather.6.cloned.1.call-update) | async-done | bytes 2097168 | tf_op jit(solution)/shard_map/all_gather | solution.py:73
  70.9 4.5 %fusion.5 = f32[512,704]{0,1:T(8,128)} fusion(bf16[512,2048]{1,0:T(8,128)(2,1)} %bitcast.128, bf16[1,704,2048]{2,1,0:T(8,128)(2,1)S(1)} %copy-done), kind=kOutput, calls=%fused_computation.14 | convolution fusion | flops 1476395008 | bytes 6422528 | tf_op jit(solution)/shard_map/dot_general | solution.py:30
  75.4 2.8 %fusion.8 = f32[512,704]{0,1:T(8,128)} fusion(bf16[512,2048]{1,0:T(8,128)(2,1)S(1)} %bitcast.131, bf16[1,704,2048]{2,1,0:T(8,128)(2,1)S(1)} %copy-done.42), kind=kOutput, calls=%fused_computation.17 | convolution fusion | flops 1476395008 | bytes 6422528 | tf_op jit(solution)/shard_map/dot_general | solution.py:30
  78.2 29.5 %all-gather.4.cloned.1.call-done = bf16[8,64,2048]{2,1,0:T(8,128)(2,1)} async-done(((bf16[8,64,512]{2,1,0:T(8,128)(2,1)}), bf16[8,64,2048]{2,1,0:T(8,128)(2,1)}) %all-gather.4.cloned.1.call-update) | async-done | bytes 2097168 | tf_op jit(solution)/shard_map/all_gather | solution.py:74
  107.8 5.4 %multiply_convert_fusion.1 = (bf16[512,704]{0,1:T(8,128)(2,1)S(1)}, bf16[512,704]{0,1:T(8,128)(2,1)S(1)}) fusion(f32[512,704]{0,1:T(8,128)} %fusion.5, f32[512,704]{0,1:T(8,128)} %fusion.8, bf16[512,2048]{1,0:T(8,128)(2,1)} %bitcast.132, bf16[1,704,2048]{2,1,0:T(8,128)(2,1)} %param.21), kind=kOutput, calls=%fused_computation.52 | convolution fusion | flops 1481080832 | bytes 9306112 | tf_op jit(solution)/shard_map/dot_general | solution.py:30
  113.2 1.9 fusion.3
  115.5 3.3 %add_convert_fusion = bf16[512,2048]{1,0:T(8,128)(2,1)} fusion(f32[512,2048]{1,0:T(8,128)S(1)} %fusion.3, bf16[512,704]{0,1:T(8,128)(2,1)S(1)} %get-tuple-element.13, bf16[1,704,2048]{2,1,0:T(8,128)(2,1)S(1)} %copy-done.43), kind=kOutput, calls=%fused_computation.5 | convolution fusion | flops 1478492160 | bytes 9895936 | tf_op jit(solution)/shard_map/dot_general | solution.py:95
  119.4 34.8 %reduce-scatter.3.cloned.1.call-done = bf16[512,512]{1,0:T(8,128)(2,1)} async-done(((bf16[512,2048]{1,0:T(8,128)(2,1)}), bf16[512,512]{1,0:T(8,128)(2,1)}) %reduce-scatter.3.cloned.1.call-update) | async-done | bytes 524304 | tf_op jit(solution)/shard_map/reduce_scatter | solution.py:98
  154.2 4.6 %all-to-all-start.2 = ((bf16[8,64,512]{2,1,0:T(8,128)(2,1)}), bf16[8,64,512]{2,1,0:T(8,128)(2,1)S(1)}, u32[]{:S(2)}, u32[]{:S(2)}) async-start(bf16[8,64,512]{2,1,0:T(8,128)(2,1)} %bitcast.91), calls=%async_computation.3 | async-start | bytes 1048576 | tf_op jit(solution)/shard_map/all_to_all | solution.py:102
  160.2 5.1 %fusion.1 = bf16[1,704,2048]{2,1,0:T(8,128)(2,1)} fusion(bf16[512,704]{0,1:T(8,128)(2,1)} %copy-done.45, bf16[512,2048]{1,0:T(8,128)(2,1)} %bitcast.129), kind=kOutput, calls=%fused_computation.10 | convolution fusion | flops 1477836800 | bytes 5701632 | tf_op jit(solution)/shard_map/dot_general | solution.py:24
  165.2 8.9 %all-to-all-done.2 = bf16[8,64,512]{2,1,0:T(8,128)(2,1)S(1)} async-done(((bf16[8,64,512]{2,1,0:T(8,128)(2,1)}), bf16[8,64,512]{2,1,0:T(8,128)(2,1)S(1)}, u32[]{:S(2)}, u32[]{:S(2)}) %all-to-all-start.2) | async-done | bytes 524320 | tf_op jit(solution)/shard_map/all_to_all | solution.py:102
  174.1 1.9 gather_fusion
  178.7 10.5 %all_gather.14 = bf16[128,2048]{1,0:T(8,128)(2,1)S(1)} all-gather(bf16[128,512]{1,0:T(8,128)(2,1)S(1)} %fusion.18), channel_id=1, replica_groups=mesh['sp'=8,'tp'=4] {'tp'}, dimensions={1}, use_global_device_ids=true | all-gather | bytes 655360 | tf_op jit(solution)/shard_map/all_gather | solution.py:115
  189.2 1.6 convolution_convert_fusion.3
  190.8 5.7 %fusion.2 = bf16[1,704,2048]{2,1,0:T(8,128)(2,1)} fusion(bf16[512,2048]{1,0:T(8,128)(2,1)} %bitcast.133, f32[512,704]{0,1:T(8,128)} %fusion.8, f32[512,704]{0,1:T(8,128)} %fusion.5), kind=kOutput, calls=%fused_computation.11 | convolution fusion | flops 1479999488 | bytes 7864320 | tf_op jit(solution)/shard_map/dot_general | solution.py:24
  196.6 2.3 fusion.125
  198.9 8.9 %all-reduce = (f32[128]{0:T(128)S(1)}, f32[128]{0:T(128)S(1)}) all-reduce(f32[128]{0:T(128)S(1)} %get-tuple-element.8, f32[128]{0:T(128)S(1)} %get-tuple-element.7), channel_id=1, replica_groups=mesh['sp'=8,'tp'=4] {'tp'}, use_global_device_ids=true, to_apply=%region_10.11 | all-reduce | flops 256 | bytes 2048 | tf_op jit(solution)/shard_map/psum | solution.py:132
  210.5 5.1 %fusion = bf16[1,704,2048]{2,1,0:T(8,128)(2,1)} fusion(bf16[512,704]{0,1:T(8,128)(2,1)} %copy-done.1, bf16[512,2048]{1,0:T(8,128)(2,1)} %bitcast.130), kind=kOutput, calls=%fused_computation.9 | convolution fusion | flops 1477836800 | bytes 5701632 | tf_op jit(solution)/shard_map/dot_general | solution.py:24
  217.6 3.5 %reduce-scatter.5.cloned.1.call-done = bf16[256,256]{1,0:T(8,128)(2,1)} async-done(((bf16[2048,256]{1,0:T(8,128)(2,1)}), bf16[256,256]{1,0:T(8,128)(2,1)}) %reduce-scatter.5.cloned.1.call-update) | async-done | bytes 131088 | tf_op jit(solution)/shard_map/reduce_scatter | solution.py:127
  221.1 1.6 convert_element_type.92
  (133 shorter events, 13.1 us)
Async XLA Ops:
  8.0 62.9 %copy-start = (bf16[1,704,2048]{2,1,0:T(8,128)(2,1)S(1)}, bf16[1,704,2048]{2,1,0:T(8,128)(2,1)}, u32[]{:S(2)}) copy-start(bf16[1,704,2048]{2,1,0:T(8,128)(2,1)} %param.19) | copy-start | bytes 8650756
  8.0 28.8 %copy-start.40 = (f32[128,2]{0,1:T(2,128)S(1)}, f32[128,2]{0,1:T(2,128)}, u32[]{:S(2)}) copy-start(f32[128,2]{0,1:T(2,128)} %param.18) | copy-start | bytes 3076
  8.0 29.0 %copy-start.3 = (bf16[128,512]{1,0:T(8,128)(2,1)S(1)}, bf16[128,512]{1,0:T(8,128)(2,1)}, u32[]{:S(2)}) copy-start(bf16[128,512]{1,0:T(8,128)(2,1)} %param.16) | copy-start | bytes 393220
  8.0 62.8 %all-gather.6.cloned.1.call-start = ((), (), s32[]{:S(2)}) async-start(), calls=%async_computation.6 | async-start | bytes 2621440 | tf_op jit(solution)/shard_map/all_gather | solution.py:73
  36.7 71.0 %all-gather.4.cloned.1.call-start = ((), (), s32[]{:S(2)}) async-start(), calls=%async_computation.5 | async-start | bytes 2621440 | tf_op jit(solution)/shard_map/all_gather | solution.py:74
  58.4 95.8 %reduce-scatter.3.cloned.1.call-start = ((), (), s32[]{:S(2)}) async-start(), calls=%async_computation.7 | async-start | bytes 2621440 | tf_op jit(solution)/shard_map/reduce_scatter | solution.py:98
  118.8 40.0 %copy-start.8 = (bf16[31,256]{1,0:T(8,128)(2,1)S(1)}, bf16[31,256]{1,0:T(8,128)(2,1)}, u32[]{:S(2)}) copy-start(bf16[31,256]{1,0:T(8,128)(2,1)} %param.28) | copy-start | bytes 47620
  118.8 77.7 %all-gather.8.cloned.1.call-start = ((), (), s32[]{:S(2)}) async-start(), calls=%async_computation.9 | async-start | bytes 1179648 | tf_op jit(solution)/shard_map/all_gather | solution.py:123
  154.2 19.9 %all-to-all-start.2 = ((bf16[8,64,512]{2,1,0:T(8,128)(2,1)}), bf16[8,64,512]{2,1,0:T(8,128)(2,1)S(1)}, u32[]{:S(2)}, u32[]{:S(2)}) async-start(bf16[8,64,512]{2,1,0:T(8,128)(2,1)} %bitcast.91), calls=%async_computation.3 | async-start | bytes 1048576 | tf_op jit(solution)/shard_map/all_to_all | solution.py:102
  158.8 62.3 %reduce-scatter.5.cloned.1.call-start = ((), (), s32[]{:S(2)}) async-start(), calls=%async_computation.8 | async-start | bytes 1179648 | tf_op jit(solution)/shard_map/reduce_scatter | solution.py:127
  177.3 11.9 %copy-start.4 = (bf16[128,256]{1,0:T(8,128)(2,1)S(1)}, bf16[128,256]{1,0:T(8,128)(2,1)}, u32[]{:S(2)}) copy-start(bf16[128,256]{1,0:T(8,128)(2,1)} %param.24) | copy-start | bytes 196612
  177.3 11.9 %copy-start.36 = (f32[128]{0:T(128)S(1)}, f32[128]{0:T(128)}, u32[]{:S(2)}) copy-start(f32[128]{0:T(128)} %param.26) | copy-start | bytes 1540
  177.3 11.9 %copy-start.38 = (f32[128]{0:T(128)S(1)}, f32[128]{0:T(128)}, u32[]{:S(2)}) copy-start(f32[128]{0:T(128)} %param.25) | copy-start | bytes 1540
  177.3 11.9 %copy-start.41 = (f32[256]{0:T(256)S(1)}, f32[256]{0:T(256)}, u32[]{:S(2)}) copy-start(f32[256]{0:T(256)} %param.27) | copy-start | bytes 3076
  178.7 17.9 %copy-start.2 = (bf16[128,512]{1,0:T(8,128)(2,1)}, bf16[128,512]{1,0:T(8,128)(2,1)S(1)}, u32[]{:S(2)}) copy-start(bf16[128,512]{1,0:T(8,128)(2,1)S(1)} %fusion.18) | copy-start | bytes 393220
  196.6 11.2 %copy-start.5 = (bf16[128,256]{1,0:T(8,128)(2,1)S(1)}, bf16[128,256]{1,0:T(8,128)(2,1)}, u32[]{:S(2)}) copy-start(bf16[128,256]{1,0:T(8,128)(2,1)} %param.24) | copy-start | bytes 196612
  196.6 11.2 %copy-start.37 = (f32[128]{0:T(128)S(1)}, f32[128]{0:T(128)}, u32[]{:S(2)}) copy-start(f32[128]{0:T(128)} %param.26) | copy-start | bytes 1540
  196.6 11.2 %copy-start.39 = (f32[128]{0:T(128)S(1)}, f32[128]{0:T(128)}, u32[]{:S(2)}) copy-start(f32[128]{0:T(128)} %param.25) | copy-start | bytes 1540
  208.9 6.7 %copy-start.6 = (bf16[128,256]{1,0:T(8,128)(2,1)S(1)}, bf16[128,256]{1,0:T(8,128)(2,1)}, u32[]{:S(2)}) copy-start(bf16[128,256]{1,0:T(8,128)(2,1)} %param.23) | copy-start | bytes 196612
  208.9 6.7 %copy-start.7 = (bf16[128,256]{1,0:T(8,128)(2,1)S(1)}, bf16[128,256]{1,0:T(8,128)(2,1)}, u32[]{:S(2)}) copy-start(bf16[128,256]{1,0:T(8,128)(2,1)} %param.22) | copy-start | bytes 196612
  208.9 6.7 %copy-start.9 = (f32[1,256]{1,0:T(1,128)S(1)}, f32[1,256]{1,0:T(1,128)}, u32[]{:S(2)}) copy-start(f32[1,256]{1,0:T(1,128)} %get-tuple-element.40) | copy-start | bytes 3076
  208.9 6.7 %copy-start.10 = (f32[1,256]{1,0:T(1,128)S(1)}, f32[1,256]{1,0:T(1,128)}, u32[]{:S(2)}) copy-start(f32[1,256]{1,0:T(1,128)} %get-tuple-element.41) | copy-start | bytes 3076
  208.9 6.6 %copy-start.11 = (f32[1,256]{1,0:T(1,128)S(1)}, f32[1,256]{1,0:T(1,128)}, u32[]{:S(2)}) copy-start(f32[1,256]{1,0:T(1,128)} %get-tuple-element.42) | copy-start | bytes 3076
  209.2 6.4 %collective-permute-start = (f32[30,256]{1,0:T(8,128)S(1)}, f32[30,256]{1,0:T(8,128)S(1)}, u32[]{:S(2)}, u32[]{:S(2)}) collective-permute-start(f32[30,256]{1,0:T(8,128)S(1)} %slice.274), channel_id=1, source_target_pairs={{4,0},{8,4},{12,8},{16,12},{20,16},{24,20},{28,24},{5,1},{9,5},{13... | collective-permute-start | bytes 92168 | tf_op jit(solution)/shard_map/ppermute | solution.py:10
  (29 other events, 174.8 us)
Sparse Core Ops, SparseCore 0:
  36.9 33.9 all-gather.5
  72.7 35.0 all-gather.3
  119.0 35.1 reduce-scatter.2
Sparse Core Ops, SparseCore 1:
  120.9 22.1 all-gather.7
  190.9 30.2 reduce-scatter.4
where the time goes:
time: 231 us; the launch traced here: 230 us
  waiting for transfers between devices  89.5 us (39%)
  blocking collectives  59.4 us (26%)
  matrix products  37.7 us (16%)
  between operations  15.9 us (7%)
  local copies, waits for them, and re-layouts  11.3 us (5%)
  other arithmetic  9.76 us (4%)
  starting transfers between devices  6.28 us (3%)
    reduce_scatter x1, waiting for transfers between devices, shards(): lax.psum_scatter(partial_value.astype(jnp.bfloat16), 'tp', scatter_dimens...  34.8 us
    all_gather x1, waiting for transfers between devices, shards(): lax.all_gather(part_cotan, 'tp', axis=2, tiled=True)  29.5 us
    all_to_all x1, blocking collectives, shards(): lax.all_to_all(rows_buf, 'sp', split_axis=0, concat_axis=0, tiled=True)  21.6 us
    all_to_all x1, blocking collectives, shards(): lax.all_to_all(cotan_buf, 'sp', split_axis=0, concat_axis=0, tiled=True)  18.4 us
    dot_general x4, matrix products, contract_rows(): lax.dot_general(left, right, (((0,), (0,)), ((), ())), preferred_element_...  17.5 us
    dot_general x3, matrix products, contract_cols(): lax.dot_general(left, right, (((1,), (1,)), ((), ())), preferred_element_...  12.7 us
    all_gather x1, waiting for transfers between devices, shards(): lax.all_gather(part_rows, 'tp', axis=2, tiled=True)  12.3 us
    all_gather x1, blocking collectives, shards(): full_stream = lax.all_gather(stream, 'tp', axis=1, tiled=True)  10.5 us
  transfers between devices with their start and end apart: 7, of which 5 were waited for; matrix products, arithmetic and copies ran while one was open for 17% of the time, Pallas kernels for 0%

commit v1 on v0

--- a/solution.py
+++ b/solution.py
@@ -1,6 +1,10 @@
+import functools
+
 import jax
 import jax.numpy as jnp
 from jax import lax
+from jax.experimental import pallas as pl
+from jax.experimental.pallas import tpu as pltpu
 from jax.sharding import PartitionSpec as P
 
 
@@ -32,7 +36,7 @@
     )
 
 
-def shards(
+def plain_shards(
     moe_input,
     cotangent,
     routes,
@@ -151,6 +155,590 @@
     return (gate_g[None], up_g[None], down_g[None], proj_g, stream, value_g, gating_g)
 
 
+VMEM = pl.BlockSpec(memory_space=pltpu.VMEM)
+
+
+def remote(src, dst, send_sem, recv_sem, sp, tp):
+    return pltpu.make_async_remote_copy(
+        src_ref=src,
+        dst_ref=dst,
+        send_sem=send_sem,
+        recv_sem=recv_sem,
+        device_id={"sp": sp, "tp": tp},
+        device_id_type=pl.DeviceIdType.MESH,
+    )
+
+
+def greet(peers):
+    barrier = pltpu.get_barrier_semaphore()
+    for sp, tp in peers:
+        pl.semaphore_signal(
+            barrier, inc=1, device_id={"sp": sp, "tp": tp}, device_id_type=pl.DeviceIdType.MESH
+        )
+    pl.semaphore_wait(barrier, len(peers))
+
+
+def rows_of(ref, index, count):
+    return ref.at[pl.ds(pl.multiple_of(index * count, count), count)]
+
+
+class ChipGather:
+    def __init__(self, own, everyone, sems, me, tp, count):
+        self.own, self.everyone, self.me, self.tp, self.count = own, everyone, me, tp, count
+        self.send, self.recv, self.relay, self.local = sems
+        self.partner = me + 1 - 2 * (me % 2)
+        self.ahead = [(me + 2 * e) % count for e in range(1, count // 2)]
+        self.behind = [(me + count - 2 * e) % count for e in range(1, count // 2)]
+
+    def block(self, index):
+        return rows_of(self.everyone, index, self.own.shape[0])
+
+    def first(self, target):
+        return remote(
+            self.own,
+            self.block(self.me),
+            self.send.at[target],
+            self.recv.at[self.me],
+            target,
+            self.tp,
+        )
+
+    def onward(self, origin):
+        return remote(
+            self.block(origin),
+            self.block(origin),
+            self.relay.at[origin],
+            self.recv.at[origin],
+            self.partner,
+            self.tp,
+        )
+
+    def start(self):
+        pltpu.make_async_copy(self.own, self.block(self.me), self.local).start()
+        for target in self.ahead + [self.partner]:
+            self.first(target).start()
+
+    def pass_on(self):
+        for origin in self.behind:
+            self.onward(origin).wait_recv()
+            self.onward(origin).start()
+
+    def finish(self):
+        pltpu.make_async_copy(self.own, self.block(self.me), self.local).wait()
+        for step in range(self.count // 2):
+            origin = (self.partner + 2 * step) % self.count
+            self.onward(origin).wait_recv()
+        for target in self.ahead + [self.partner]:
+            self.first(target).wait_send()
+        for origin in self.behind:
+            self.onward(origin).wait_send()
+
+
+def gather_sems(count):
+    return [
+        pltpu.SemaphoreType.DMA((count,)),
+        pltpu.SemaphoreType.DMA((count,)),
+        pltpu.SemaphoreType.DMA((count,)),
+        pltpu.SemaphoreType.DMA,
+    ]
+
+
+def dispatch_kernel(
+    count, rows, cot, mixed, rows_out, cot_out, mixed_out, send, recv, local, *mixed_sems
+):
+    me, tp = lax.axis_index("sp"), lax.axis_index("tp")
+    capacity, width = rows.shape[1:]
+    across, down, corner = tp + 1 - 2 * (tp % 2), (tp + 2) % 4, 3 - tp
+    others = [(me + d) % count for d in range(1, count)]
+    greet([(other, tp) for other in others] + [(me, across), (me, down)])
+    arrays = ((rows, rows_out), (cot, cot_out))
+
+    def block(a, source, owner):
+        return arrays[a][1].at[
+            pl.ds(pl.multiple_of(source * capacity, capacity), capacity),
+            pl.ds(pl.multiple_of(owner * width, 128), width),
+        ]
+
+    def own_copy(a):
+        return pltpu.make_async_copy(arrays[a][0].at[me], block(a, me, tp), local.at[a])
+
+    def out_copy(a, target):
+        return remote(
+            arrays[a][0].at[target],
+            block(a, me, tp),
+            send.at[a, target, 0],
+            recv.at[a, me, tp],
+            target,
+            tp,
+        )
+
+    def side_copy(a, source, owner, target, lane):
+        spot = block(a, source, owner)
+        return remote(spot, spot, send.at[a, source, lane], recv.at[a, source, owner], me, target)
+
+    for a in range(2):
+        own_copy(a).start()
+    for target in others:
+        for a in range(2):
+            out_copy(a, target).start()
+    gather = ChipGather(mixed, mixed_out, mixed_sems, me, tp, count)
+    gather.start()
+
+    def relay_of(step):
+        return (across, down) if step % 2 == 0 else (down, across)
+
+    def relay(step):
+        source = (me + count - step) % count
+        owner, target = relay_of(step)
+        for a in range(2):
+            side_copy(a, source, owner, target, 3).wait_recv()
+            side_copy(a, source, owner, target, 3).start()
+
+    for step in range(count):
+        source = (me + count - step) % count
+        for a in range(2):
+            if step == 0:
+                own_copy(a).wait()
+            else:
+                side_copy(a, source, tp, across, 1).wait_recv()
+            side_copy(a, source, tp, across, 1).start()
+            side_copy(a, source, tp, down, 2).start()
+        if step >= 1:
+            relay(step - 1)
+    relay(count - 1)
+    gather.pass_on()
+    for step in range(count):
+        source = (me + count - step) % count
+        owner, target = relay_of(step)
+        for a in range(2):
+            side_copy(a, source, target, across, 1).wait_recv()
+            side_copy(a, source, corner, across, 1).wait_recv()
+            side_copy(a, source, tp, across, 1).wait_send()
+            side_copy(a, source, tp, down, 2).wait_send()
+            side_copy(a, source, owner, target, 3).wait_send()
+    for target in others:
+        for a in range(2):
+            out_copy(a, target).wait_send()
+    gather.finish()
+
+
+def dispatch(rows, cot, mixed, count):
+    capacity, width = rows.shape[1:]
+    full = jax.ShapeDtypeStruct((count * capacity, width * lax.axis_size("tp")), jnp.bfloat16)
+    return pl.pallas_call(
+        functools.partial(dispatch_kernel, count),
+        out_shape=(
+            full,
+            full,
+            jax.ShapeDtypeStruct((count * mixed.shape[0], mixed.shape[1]), mixed.dtype),
+        ),
+        in_specs=[VMEM] * 3,
+        out_specs=(VMEM,) * 3,
+        scratch_shapes=[
+            pltpu.SemaphoreType.DMA((2, count, 4)),
+            pltpu.SemaphoreType.DMA((2, count, 4)),
+            pltpu.SemaphoreType.DMA((2,)),
+        ]
+        + gather_sems(count),
+        compiler_params=pltpu.CompilerParams(
+            collective_id=0, has_side_effects=True, vmem_limit_bytes=40 << 20
+        ),
+        name="dispatch",
+    )(rows, cot, mixed)
+
+
+def combine_kernel(
+    count,
+    partial_ref,
+    cot,
+    pick,
+    proj,
+    stream,
+    proj_out,
+    landed,
+    reduced,
+    back,
+    send,
+    recv,
+    back_send,
+    back_recv,
+    wide_send,
+    wide_recv,
+    *proj_sems,
+):
+    me, tp = lax.axis_index("sp"), lax.axis_index("tp")
+    capacity, width = reduced.shape[1:]
+    group = (tp + 1 - 2 * (tp % 2), (tp + 2) % 4, 3 - tp)
+    others = [(me + d) % count for d in range(1, count)]
+    greet([(other, tp) for other in others] + [(me, other) for other in group])
+
+    def share(source, owner):
+        return partial_ref.at[
+            pl.ds(pl.multiple_of(source * capacity, capacity), capacity),
+            pl.ds(pl.multiple_of(owner * width, 128), width),
+        ]
+
+    def share_copy(source, q):
+        return remote(
+            share(source, group[q]),
+            landed.at[q, source],
+            send.at[source, q],
+            recv.at[source, q],
+            me,
+            group[q],
+        )
+
+    def back_copy(target):
+        return remote(
+            reduced.at[target],
+            rows_of(back, me, capacity),
+            back_send.at[target],
+            back_recv.at[me],
+            target,
+            tp,
+        )
+
+    order = others + [me]
+    for source in order:
+        for q in range(3):
+            share_copy(source, q).start()
+    gather = ChipGather(proj, proj_out, proj_sems, me, tp, count)
+    gather.start()
+    for step, source in enumerate(order):
+        total = share(source, tp)[...].astype(jnp.float32)
+        for q in range(3):
+            share_copy(source, q).wait_recv()
+            total = total + landed[q, source].astype(jnp.float32)
+        total = total.astype(jnp.bfloat16)
+        if step < count - 1:
+            reduced[source] = total
+            back_copy(source).start()
+        else:
+            back[pl.ds(pl.multiple_of(me * capacity, capacity), capacity), :] = total
+    gather.pass_on()
+    for other in others:
+        remote(
+            reduced.at[other],
+            rows_of(back, other, capacity),
+            back_send.at[other],
+            back_recv.at[other],
+            other,
+            tp,
+        ).wait_recv()
+    mine = jnp.dot(pick[...], back[...], preferred_element_type=jnp.float32)
+    columns = pl.ds(pl.multiple_of(tp * width, 128), width)
+    stream[:, columns] = (cot[...].astype(jnp.float32) + mine).astype(jnp.bfloat16)
+
+    def wide_copy(q):
+        spot = stream.at[:, columns]
+        return remote(spot, spot, wide_send.at[q], wide_recv.at[q], me, group[q])
+
+    for q in range(3):
+        wide_copy(q).start()
+    for q in range(3):
+        wide_copy(q).wait()
+    for source in order:
+        for q in range(3):
+            share_copy(source, q).wait_send()
+    for other in others:
+        back_copy(other).wait_send()
+    gather.finish()
+
+
+def combine(partial_value, cot, pick, proj, count):
+    tokens, width = cot.shape
+    capacity = partial_value.shape[0] // count
+    return pl.pallas_call(
+        functools.partial(combine_kernel, count),
+        out_shape=(
+            jax.ShapeDtypeStruct((tokens, partial_value.shape[1]), jnp.bfloat16),
+            jax.ShapeDtypeStruct((count * proj.shape[0], proj.shape[1]), jnp.bfloat16),
+        ),
+        in_specs=[VMEM] * 4,
+        out_specs=(VMEM,) * 2,
+        scratch_shapes=[
+            pltpu.VMEM((3, count, capacity, width), jnp.bfloat16),
+            pltpu.VMEM((count, capacity, width), jnp.bfloat16),
+            pltpu.VMEM((count * capacity, width), jnp.bfloat16),
+            pltpu.SemaphoreType.DMA((count, 3)),
+            pltpu.SemaphoreType.DMA((count, 3)),
+            pltpu.SemaphoreType.DMA((count,)),
+            pltpu.SemaphoreType.DMA((count,)),
+            pltpu.SemaphoreType.DMA((3,)),
+            pltpu.SemaphoreType.DMA((3,)),
+        ]
+        + gather_sems(count),
+        compiler_params=pltpu.CompilerParams(
+            collective_id=1, has_side_effects=True, vmem_limit_bytes=40 << 20
+        ),
+        name="combine",
+    )(partial_value, cot, pick, proj)
+
+
+def module_kernel(
+    count,
+    stream,
+    proj,
+    mixed,
+    conv_out,
+    row_mean,
+    row_rstd,
+    gain,
+    taps,
+    v_value,
+    v_gate,
+    proj_grad,
+    value_grad,
+    gating_grad,
+    columns,
+    sums,
+    arrived,
+    extended,
+    send,
+    recv,
+    local,
+    sum_send,
+    sum_recv,
+    edge_send,
+    edge_recv,
+):
+    me, tp = lax.axis_index("sp"), lax.axis_index("tp")
+    tokens, channels = conv_out.shape
+    depth = stream.shape[1] // count
+    halo = extended.shape[0] - tokens
+    group = (tp + 1 - 2 * (tp % 2), (tp + 2) % 4, 3 - tp)
+    others = [(me + d) % count for d in range(1, count)]
+    greet([(other, tp) for other in others] + [(me, other) for other in group])
+
+    def strip(index):
+        return stream.at[:, pl.ds(pl.multiple_of(index * depth, 128), depth)]
+
+    def strip_copy(target):
+        return remote(
+            strip(target),
+            rows_of(columns, me, tokens),
+            send.at[target],
+            recv.at[me],
+            target,
+            tp,
+        )
+
+    own = pltpu.make_async_copy(strip(me), rows_of(columns, me, tokens), local)
+    own.start()
+    for other in others:
+        strip_copy(other).start()
+    mixed_grad = jnp.dot(stream[...], proj[...], preferred_element_type=jnp.float32)
+    normed = (conv_out[...].astype(jnp.float32) - row_mean[...]) * row_rstd[...]
+    scaled = normed * gain[...]
+    sig = jax.nn.sigmoid(scaled)
+    norm_grad = mixed_grad * sig * (1.0 + scaled * (1.0 - sig)) * gain[...]
+    first = jnp.sum(norm_grad, axis=1, keepdims=True)
+    second = jnp.sum(norm_grad * normed, axis=1, keepdims=True)
+    lanes = lax.broadcasted_iota(jnp.int32, (tokens, 128), 1)
+    pair = jnp.where(lanes % 2 == 0, first, second)
+    sums[...] = pair.T[:8]
+
+    def sum_copy(q):
+        return remote(sums, arrived.at[q], sum_send.at[q], sum_recv.at[q], me, group[q])
+
+    for q in range(3):
+        sum_copy(q).start()
+    value_sig = jax.nn.sigmoid(v_gate[...].astype(jnp.float32))
+    gating_scale = v_value[...].astype(jnp.float32) * value_sig * (1.0 - value_sig)
+    for q in range(3):
+        sum_copy(q).wait()
+    total = sums[...] + arrived[0] + arrived[1] + arrived[2]
+    total = total * (1.0 / (channels * 4))
+    means = jnp.concatenate([total] * 16, axis=0).T
+    conv_grad = row_rstd[...] * (norm_grad - means[:, 0:1] - normed * means[:, 1:2])
+    extended[:tokens] = conv_grad
+    edge = remote(
+        extended.at[pl.ds(0, halo)],
+        extended.at[pl.ds(tokens, halo)],
+        edge_send,
+        edge_recv,
+        (me + count - 1) % count,
+        tp,
+    )
+
+    @pl.when(me > 0)
+    def _():
+        edge.start()
+
+    @pl.when(me == count - 1)
+    def _():
+        extended[tokens:] = jnp.zeros((halo, channels), jnp.float32)
+
+    @pl.when(me < count - 1)
+    def _():
+        edge.wait_recv()
+
+    kernel = taps.shape[0]
+    unit_grad = jnp.zeros((tokens, channels), jnp.float32)
+    for offset in range(kernel):
+        lead = kernel - 1 - offset
+        tap = taps[offset : offset + 1, :].astype(jnp.float32)
+        unit_grad = unit_grad + tap * extended[lead : lead + tokens, :]
+    value_grad[...] = (unit_grad * value_sig).astype(jnp.bfloat16)
+    gating_grad[...] = (unit_grad * gating_scale).astype(jnp.bfloat16)
+    own.wait()
+    for other in others:
+        remote(
+            strip(other),
+            rows_of(columns, other, tokens),
+            send.at[other],
+            recv.at[other],
+            other,
+            tp,
+        ).wait_recv()
+    proj_grad[...] = contract_rows(columns[...], mixed[...])
+    for other in others:
+        strip_copy(other).wait_send()
+
+    @pl.when(me > 0)
+    def _():
+        edge.wait_send()
+
+
+def module(stream, proj, mixed, conv_out, row_mean, row_rstd, gain, taps, v_value, v_gate, count):
+    tokens, channels = conv_out.shape
+    depth = stream.shape[1] // count
+    halo = -(-(taps.shape[0] - 1) // 8) * 8
+    return pl.pallas_call(
+        functools.partial(module_kernel, count),
+        out_shape=(
+            jax.ShapeDtypeStruct((depth, channels), jnp.float32),
+            jax.ShapeDtypeStruct((tokens, channels), jnp.bfloat16),
+            jax.ShapeDtypeStruct((tokens, channels), jnp.bfloat16),
+        ),
+        in_specs=[VMEM] * 10,
+        out_specs=(VMEM,) * 3,
+        scratch_shapes=[
+            pltpu.VMEM((count * tokens, depth), jnp.bfloat16),
+            pltpu.VMEM((8, tokens), jnp.float32),
+            pltpu.VMEM((3, 8, tokens), jnp.float32),
+            pltpu.VMEM((tokens + halo, channels), jnp.float32),
+            pltpu.SemaphoreType.DMA((count,)),
+            pltpu.SemaphoreType.DMA((count,)),
+            pltpu.SemaphoreType.DMA,
+            pltpu.SemaphoreType.DMA((3,)),
+            pltpu.SemaphoreType.DMA((3,)),
+            pltpu.SemaphoreType.DMA,
+            pltpu.SemaphoreType.DMA,
+        ],
+        compiler_params=pltpu.CompilerParams(
+            collective_id=2, has_side_effects=True, vmem_limit_bytes=40 << 20
+        ),
+        name="module",
+    )(stream, proj, mixed, conv_out, row_mean, row_rstd, gain, taps, v_value, v_gate)
+
+
+def kernel_shards(
+    moe_input,
+    cotangent,
+    routes,
+    route_weight,
+    w_gate,
+    w_up,
+    w_down,
+    v_value,
+    v_gate,
+    conv_out,
+    row_mean,
+    row_rstd,
+    ln_gain,
+    taps,
+    out_proj,
+):
+    experts = lax.axis_size("sp")
+    tokens, width = moe_input.shape
+    capacity = 4 * tokens // experts
+    total = experts * capacity
+    flat_routes = routes.reshape(-1)
+    member = (flat_routes[:, None] == jnp.arange(experts, dtype=jnp.int32)[None, :]).astype(
+        jnp.bfloat16
+    )
+    index = jnp.arange(2 * tokens, dtype=jnp.int32)
+    before = (index[None, :] < index[:, None]).astype(jnp.bfloat16)
+    earlier = jnp.dot(before, member, preferred_element_type=jnp.float32)
+    slot_index = jnp.sum(earlier * member.astype(jnp.float32), axis=1).astype(jnp.int32)
+    buffer_row = (flat_routes * capacity + slot_index).reshape(tokens, 2)
+    places = jnp.arange(total, dtype=jnp.int32)
+    place0 = (buffer_row[:, 0][:, None] == places[None, :]).astype(jnp.bfloat16)
+    place1 = (buffer_row[:, 1][:, None] == places[None, :]).astype(jnp.bfloat16)
+    pick = place0 + place1
+    cot32 = cotangent.astype(jnp.float32)
+    weighted = jnp.concatenate(
+        [
+            (route_weight[:, 0:1] * cot32).astype(jnp.bfloat16),
+            (route_weight[:, 1:2] * cot32).astype(jnp.bfloat16),
+        ],
+        axis=0,
+    )
+    rows_buf = contract_rows(pick, moe_input).astype(jnp.bfloat16)
+    cot_buf = contract_rows(jnp.concatenate([place0, place1], axis=0), weighted).astype(
+        jnp.bfloat16
+    )
+    normed = (conv_out.astype(jnp.float32) - row_mean[:, None]) * row_rstd[:, None]
+    scaled_norm = normed * ln_gain[None, :]
+    mixed = (scaled_norm * jax.nn.sigmoid(scaled_norm)).astype(jnp.bfloat16)
+    expert_in, expert_cot, mixed_all = dispatch(
+        rows_buf.reshape(experts, capacity, width),
+        cot_buf.reshape(experts, capacity, width),
+        mixed,
+        experts,
+    )
+    gate_w = w_gate[0]
+    up_w = w_up[0]
+    down_w = w_down[0]
+    gate_pre = contract_cols(expert_in, gate_w)
+    up_pre = contract_cols(expert_in, up_w)
+    gate_sig = jax.nn.sigmoid(gate_pre)
+    gate_act = gate_pre * gate_sig
+    hidden = (gate_act * up_pre).astype(jnp.bfloat16)
+    hidden_grad = contract_cols(expert_cot, down_w)
+    gate_delta = (hidden_grad * up_pre * gate_sig * (1.0 + gate_pre * (1.0 - gate_sig))).astype(
+        jnp.bfloat16
+    )
+    up_delta = (hidden_grad * gate_act).astype(jnp.bfloat16)
+    partial_value = jnp.dot(gate_delta, gate_w, preferred_element_type=jnp.float32) + jnp.dot(
+        up_delta, up_w, preferred_element_type=jnp.float32
+    )
+    stream_full, proj_full = combine(
+        partial_value.astype(jnp.bfloat16), cotangent, pick, out_proj, experts
+    )
+    down_g = contract_rows(hidden, expert_cot).astype(jnp.bfloat16)
+    gate_g = contract_rows(gate_delta, expert_in).astype(jnp.bfloat16)
+    up_g = contract_rows(up_delta, expert_in).astype(jnp.bfloat16)
+    proj_g, value_g, gating_g = module(
+        stream_full,
+        proj_full,
+        mixed_all,
+        conv_out,
+        row_mean[:, None],
+        row_rstd[:, None],
+        ln_gain[None, :],
+        taps,
+        v_value,
+        v_gate,
+        experts,
+    )
+    stream = lax.dynamic_slice_in_dim(stream_full, lax.axis_index("tp") * width, width, 1)
+    return (gate_g[None], up_g[None], down_g[None], proj_g, stream, value_g, gating_g)
+
+
+def shards(*blocks):
+    tokens, width = blocks[0].shape
+    depth, channels = blocks[-1].shape
+    experts = lax.axis_size("sp")
+    square = lax.axis_size("tp") == 4 and experts % 2 == 0 and tokens == 128
+    capacity = 4 * tokens // experts
+    tiled = width % 128 == 0 and depth % 128 == 0 and channels % 128 == 0 and capacity % 16 == 0
+    if square and tiled:
+        return kernel_shards(*blocks)
+    return plain_shards(*blocks)
+
+
 def solution(mesh):
     return jax.shard_map(
         shards,

time: 231 us -> 147 us (0.64)
  the two profiles are of different devices: /device:TPU:0 before, /device:TPU:13 now
where the time goes in v1:
time: 147 us
  Pallas kernels  103 us (70%)
  matrix products  22.7 us (15%)
  local copies, waits for them, and re-layouts  17.7 us (12%)
  other arithmetic  2.07 us (1%)
    pallas_call x1, Pallas kernels, combine(): pl.pallas_call(functools.partial(combine_kernel, count), out_shape=(jax.S...  43.4 us
    pallas_call x1, Pallas kernels, dispatch(): pl.pallas_call(functools.partial(dispatch_kernel, count), out_shape=(full...  43 us
    pallas_call x1, Pallas kernels, module(): pl.pallas_call(functools.partial(module_kernel, count), out_shape=(jax.Sh...  16.9 us
    unnamed x72, local copies, waits for them, and re-layouts  13.8 us
    dot_general x5, matrix products, contract_rows(): lax.dot_general(left, right, (((0,), (0,)), ((), ())), preferred_element_...  13.1 us
    dot_general x3, matrix products, contract_cols(): lax.dot_general(left, right, (((1,), (1,)), ((), ())), preferred_element_...  5.5 us

profile of v1, /device:TPU:13, one launch (start us, length us, event | category | flops | bytes accessed | tf_op | source)
XLA Modules:
  0.0 146.8 jit_solution(11058893394816312174)
XLA Ops:
  0.7 0.9 copy.34
  2.2 0.7 multiply_add_fusion
  3.0 0.8 slice_bitcast_fusion.1
  3.8 1.0 fusion.14
  5.7 43.0 %dispatch.1 = (bf16[512,2048]{1,0:T(8,128)(2,1)S(1)}, bf16[512,2048]{1,0:T(8,128)(2,1)S(1)}, bf16[1024,256]{1,0:T(8,128)(2,1)S(1)}) custom-call(bf16[8,64,512]{2,1,0:T(8,128)(2,1)S(1)} %bitcast.45, bf16[8,64,512]{2,1,0:T(8,128)(2,1)S(1)} %bitcast.46, bf16[128,256]{1,0:T(8,128)(2,1)S(1)} %multiply_convert_fusion.4.mixed), custom_call_target="tpu_custom_call" | custom-call | tf_op jit(solution)/shard_map/dispatch/pallas_call | solution.py:328
  48.8 1.7 %fusion.5 = f32[512,704]{0,1:T(8,128)S(1)} fusion(bf16[512,2048]{1,0:T(8,128)(2,1)S(1)} %get-tuple-element.16, bf16[1,704,2048]{2,1,0:T(8,128)(2,1)S(1)} %copy-done), kind=kOutput, calls=%fused_computation.9 | convolution fusion | flops 1476395008 | bytes 6422528 | tf_op jit(solution)/shard_map/dot_general | solution.py:34
  50.5 1.8 %copy-done.29 = bf16[1,704,2048]{2,1,0:T(8,128)(2,1)S(1)} copy-done((bf16[1,704,2048]{2,1,0:T(8,128)(2,1)S(1)}, bf16[1,704,2048]{2,1,0:T(8,128)(2,1)}, u32[]{:S(2)}) %copy-start.29) | copy-done | bytes 2883608
  52.3 1.7 %fusion.8 = f32[512,704]{0,1:T(8,128)S(1)} fusion(bf16[512,2048]{1,0:T(8,128)(2,1)S(1)} %get-tuple-element.16, bf16[1,704,2048]{2,1,0:T(8,128)(2,1)S(1)} %copy-done.29), kind=kOutput, calls=%fused_computation.12 | convolution fusion | flops 1476395008 | bytes 6422528 | tf_op jit(solution)/shard_map/dot_general | solution.py:34
  54.6 2.1 %multiply_convert_fusion.1 = (bf16[512,704]{0,1:T(8,128)(2,1)S(1)}, bf16[512,704]{0,1:T(8,128)(2,1)S(1)}) fusion(f32[512,704]{0,1:T(8,128)S(1)} %fusion.5, f32[512,704]{0,1:T(8,128)S(1)} %fusion.8, bf16[512,2048]{1,0:T(8,128)(2,1)S(1)} %get-tuple-element.15, bf16[1,704,2048]{2,1,0:T(8,128)(2,1)S(1)} %copy-done.28), kind=kOutput, calls=%fused_computation.17 | convolution fusion | flops 1481080832 | bytes 9306112 | tf_op jit(solution)/shard_map/dot_general | solution.py:34
  56.8 1.9 %fusion.3 = f32[512,2048]{1,0:T(8,128)S(1)} fusion(bf16[512,704]{0,1:T(8,128)(2,1)S(1)} %get-tuple-element.24, bf16[1,704,2048]{2,1,0:T(8,128)(2,1)S(1)} %copy-done), kind=kOutput, calls=%fused_computation.7 | convolution fusion | flops 1476395008 | bytes 7798784 | tf_op jit(solution)/shard_map/dot_general | solution.py:704
  58.7 2.0 %add_convert_fusion.partial_ref = bf16[512,2048]{1,0:T(8,128)(2,1)S(1)} fusion(f32[512,2048]{1,0:T(8,128)S(1)} %fusion.3, bf16[512,704]{0,1:T(8,128)(2,1)S(1)} %get-tuple-element.23, bf16[1,704,2048]{2,1,0:T(8,128)(2,1)S(1)} %copy-done.29), kind=kOutput, calls=%fused_computation | convolution fusion | flops 1478492160 | bytes 9895936 | tf_op jit(solution)/shard_map/dot_general | solution.py:704
  60.9 43.4 %combine.1 = (bf16[128,2048]{1,0:T(8,128)(2,1)S(1)}, bf16[2048,256]{1,0:T(8,128)(2,1)S(1)}) custom-call(bf16[512,2048]{1,0:T(8,128)(2,1)S(1)} %add_convert_fusion.partial_ref, bf16[128,512]{1,0:T(8,128)(2,1)S(1)} %copy-done.3, bf16[128,512]{1,0:T(8,128)(2,1)S(1)} %fusion.25.pick, bf16[256,256]{1,0:T(8,128)(2,1)S(1)} %copy-done.10), custom_call_target="tpu_custom_call" | custom-call | tf_op jit(solution)/shard_map/combine/pallas_call | solution.py:451
  104.3 1.0 copy-done.1
  105.2 0.8 copy.36.row_mean
  106.0 1.4 copy.37.row_rstd
  107.4 1.2 copy-done.2
  108.6 1.0 copy-done.5
  109.6 0.8 copy-done.7
  110.5 0.8 copy-done.11
  111.3 0.8 copy-done.12
  112.8 16.9 %module.1 = (f32[256,256]{1,0:T(8,128)S(1)}, bf16[128,256]{1,0:T(8,128)(2,1)S(1)}, bf16[128,256]{1,0:T(8,128)(2,1)S(1)}) custom-call(bf16[128,2048]{1,0:T(8,128)(2,1)S(1)} %get-tuple-element.17.stream, bf16[2048,256]{1,0:T(8,128)(2,1)S(1)} %copy-done.2, bf16[1024,256]{1,0:T(8,128)(2,1)S(1)} %copy-done.5, bf16[128,256]{1,0:T(8,128)(2,1)S(1)} %copy-done.6, ...), custom_call_target="tpu_custom_call" | custom-call | tf_op jit(solution)/shard_map/module/pallas_call | solution.py:607
  132.4 5.9 %fusion.2 = bf16[1,704,2048]{2,1,0:T(8,128)(2,1)} fusion(bf16[512,2048]{1,0:T(8,128)(2,1)} %copy-done.22, f32[512,704]{0,1:T(8,128)} %copy-done.33, f32[512,704]{0,1:T(8,128)} %copy-done.32), kind=kOutput, calls=%fused_computation.6 | convolution fusion | flops 1479999488 | bytes 7864320 | tf_op jit(solution)/shard_map/dot_general | solution.py:28
  138.3 3.2 %fusion.1 = bf16[1,704,2048]{2,1,0:T(8,128)(2,1)} fusion(bf16[512,704]{0,1:T(8,128)(2,1)S(1)} %copy-done.31, bf16[512,2048]{1,0:T(8,128)(2,1)S(1)} %copy-done.21), kind=kOutput, calls=%fused_computation.5 | convolution fusion | flops 1477836800 | bytes 5701632 | tf_op jit(solution)/shard_map/dot_general | solution.py:28
  141.6 3.3 %fusion = bf16[1,704,2048]{2,1,0:T(8,128)(2,1)} fusion(bf16[512,704]{0,1:T(8,128)(2,1)S(1)} %copy-done.24, bf16[512,2048]{1,0:T(8,128)(2,1)S(1)} %copy-done.21), kind=kOutput, calls=%fused_computation.4 | convolution fusion | flops 1477836800 | bytes 5701632 | tf_op jit(solution)/shard_map/dot_general | solution.py:28
  (76 shorter events, 7.6 us)
Async XLA Ops:
  0.6 48.2 %copy-start = (bf16[1,704,2048]{2,1,0:T(8,128)(2,1)S(1)}, bf16[1,704,2048]{2,1,0:T(8,128)(2,1)}, u32[]{:S(2)}) copy-start(bf16[1,704,2048]{2,1,0:T(8,128)(2,1)} %param.19) | copy-start | bytes 8650756
  0.6 4.5 %copy-start.25 = (bf16[128,512]{1,0:T(8,128)(2,1)S(1)}, bf16[128,512]{1,0:T(8,128)(2,1)}, u32[]{:S(2)}) copy-start(bf16[128,512]{1,0:T(8,128)(2,1)} %param.15) | copy-start | bytes 393220
  0.7 4.9 %copy-start.6 = (bf16[128,256]{1,0:T(8,128)(2,1)S(1)}, bf16[128,256]{1,0:T(8,128)(2,1)}, u32[]{:S(2)}) copy-start(bf16[128,256]{1,0:T(8,128)(2,1)} %conv_out.1) | copy-start | bytes 196612
  0.7 4.9 %copy-start.26 = (f32[128]{0:T(128)S(1)}, f32[128]{0:T(128)}, u32[]{:S(2)}) copy-start(f32[128]{0:T(128)} %param.25) | copy-start | bytes 1540
  0.7 4.9 %copy-start.27 = (f32[128]{0:T(128)S(1)}, f32[128]{0:T(128)}, u32[]{:S(2)}) copy-start(f32[128]{0:T(128)} %param.26) | copy-start | bytes 1540
  0.7 4.9 %copy-start.18 = (f32[256]{0:T(256)S(1)}, f32[256]{0:T(256)}, u32[]{:S(2)}) copy-start(f32[256]{0:T(256)} %param.27) | copy-start | bytes 3076
  48.8 1.8 %copy-start.4 = (bf16[1024,256]{1,0:T(8,128)(2,1)}, bf16[1024,256]{1,0:T(8,128)(2,1)S(1)}, u32[]{:S(2)}) copy-start(bf16[1024,256]{1,0:T(8,128)(2,1)S(1)} %get-tuple-element.19.mixed) | copy-start | bytes 1572868
  48.8 1.8 %copy-start.20 = (bf16[512,2048]{1,0:T(8,128)(2,1)}, bf16[512,2048]{1,0:T(8,128)(2,1)S(1)}, u32[]{:S(2)}) copy-start(bf16[512,2048]{1,0:T(8,128)(2,1)S(1)} %get-tuple-element.16) | copy-start | bytes 6291460
  48.8 5.2 %copy-start.22 = (bf16[512,2048]{1,0:T(8,128)(2,1)}, bf16[512,2048]{1,0:T(8,128)(2,1)S(1)}, u32[]{:S(2)}) copy-start(bf16[512,2048]{1,0:T(8,128)(2,1)S(1)} %get-tuple-element.15) | copy-start | bytes 6291460
  48.8 3.5 %copy-start.29 = (bf16[1,704,2048]{2,1,0:T(8,128)(2,1)S(1)}, bf16[1,704,2048]{2,1,0:T(8,128)(2,1)}, u32[]{:S(2)}) copy-start(bf16[1,704,2048]{2,1,0:T(8,128)(2,1)} %param.20) | copy-start | bytes 8650756
  52.3 1.7 %copy-start.32 = (f32[512,704]{0,1:T(8,128)}, f32[512,704]{0,1:T(8,128)S(1)}, u32[]{:S(2)}) copy-start(f32[512,704]{0,1:T(8,128)S(1)} %fusion.5) | copy-start | bytes 4325380
  52.3 2.3 %copy-start.28 = (bf16[1,704,2048]{2,1,0:T(8,128)(2,1)S(1)}, bf16[1,704,2048]{2,1,0:T(8,128)(2,1)}, u32[]{:S(2)}) copy-start(bf16[1,704,2048]{2,1,0:T(8,128)(2,1)} %param.21) | copy-start | bytes 8650756
  54.0 2.8 %copy-start.33 = (f32[512,704]{0,1:T(8,128)}, f32[512,704]{0,1:T(8,128)S(1)}, u32[]{:S(2)}) copy-start(f32[512,704]{0,1:T(8,128)S(1)} %fusion.8) | copy-start | bytes 4325380
  56.8 1.9 %copy-start.23 = (bf16[512,704]{0,1:T(8,128)(2,1)}, bf16[512,704]{0,1:T(8,128)(2,1)S(1)}, u32[]{:S(2)}) copy-start(bf16[512,704]{0,1:T(8,128)(2,1)S(1)} %get-tuple-element.24) | copy-start | bytes 2162692
  56.8 1.9 %copy-start.30 = (bf16[512,704]{0,1:T(8,128)(2,1)}, bf16[512,704]{0,1:T(8,128)(2,1)S(1)}, u32[]{:S(2)}) copy-start(bf16[512,704]{0,1:T(8,128)(2,1)S(1)} %get-tuple-element.23) | copy-start | bytes 2162692
  58.7 2.2 %copy-start.3 = (bf16[128,512]{1,0:T(8,128)(2,1)S(1)}, bf16[128,512]{1,0:T(8,128)(2,1)}, u32[]{:S(2)}) copy-start(bf16[128,512]{1,0:T(8,128)(2,1)} %cot.1) | copy-start | bytes 393220
  58.7 2.2 %copy-start.10 = (bf16[256,256]{1,0:T(8,128)(2,1)S(1)}, bf16[256,256]{1,0:T(8,128)(2,1)}, u32[]{:S(2)}) copy-start(bf16[256,256]{1,0:T(8,128)(2,1)} %proj.1) | copy-start | bytes 393220
  60.7 46.7 %copy-start.17 = (bf16[31,256]{1,0:T(8,128)(2,1)S(1)}, bf16[31,256]{1,0:T(8,128)(2,1)}, u32[]{:S(2)}) copy-start(bf16[31,256]{1,0:T(8,128)(2,1)} %taps.1) | copy-start | bytes 47620
  132.4 5.9 %copy-start.21 = (bf16[512,2048]{1,0:T(8,128)(2,1)S(1)}, bf16[512,2048]{1,0:T(8,128)(2,1)}, u32[]{:S(2)}) copy-start(bf16[512,2048]{1,0:T(8,128)(2,1)} %copy-done.20) | copy-start | bytes 6291460
  132.4 5.9 %copy-start.31 = (bf16[512,704]{0,1:T(8,128)(2,1)S(1)}, bf16[512,704]{0,1:T(8,128)(2,1)}, u32[]{:S(2)}) copy-start(bf16[512,704]{0,1:T(8,128)(2,1)} %copy-done.30) | copy-start | bytes 2162692
  138.3 3.2 %copy-start.24 = (bf16[512,704]{0,1:T(8,128)(2,1)S(1)}, bf16[512,704]{0,1:T(8,128)(2,1)}, u32[]{:S(2)}) copy-start(bf16[512,704]{0,1:T(8,128)(2,1)} %copy-done.23) | copy-start | bytes 2162692
  141.5 3.3 %copy-start.9 = (f32[256,256]{1,0:T(8,128)S(1)}, f32[256,256]{1,0:T(8,128)}, u32[]{:S(2)}) copy-start(f32[256,256]{1,0:T(8,128)} %copy-done.8) | copy-start | bytes 786436
  141.5 4.0 %copy-start.16 = (bf16[128,256]{1,0:T(8,128)(2,1)S(1)}, bf16[128,256]{1,0:T(8,128)(2,1)}, u32[]{:S(2)}) copy-start(bf16[128,256]{1,0:T(8,128)(2,1)} %copy-done.15) | copy-start | bytes 196612
  141.5 4.6 %copy-start.14 = (bf16[128,256]{1,0:T(8,128)(2,1)S(1)}, bf16[128,256]{1,0:T(8,128)(2,1)}, u32[]{:S(2)}) copy-start(bf16[128,256]{1,0:T(8,128)(2,1)} %copy-done.13) | copy-start | bytes 196612
  (10 other events, 8.4 us)

commit v2 on v1

--- a/solution.py
+++ b/solution.py
@@ -344,6 +344,9 @@
             collective_id=0, has_side_effects=True, vmem_limit_bytes=40 << 20
         ),
         name="dispatch",
+        cost_estimate=pl.CostEstimate(
+            flops=0, bytes_accessed=200 * rows.size * 2, transcendentals=0
+        ),
     )(rows, cot, mixed)
 
 
@@ -353,9 +356,16 @@
     cot,
     pick,
     proj,
+    hidden,
+    gate_delta,
+    up_delta,
+    expert_in,
+    expert_cot,
     stream,
     proj_out,
+    grads,
     landed,
+    middle,
     reduced,
     back,
     send,
@@ -368,7 +378,9 @@
 ):
     me, tp = lax.axis_index("sp"), lax.axis_index("tp")
     capacity, width = reduced.shape[1:]
-    group = (tp + 1 - 2 * (tp % 2), (tp + 2) % 4, 3 - tp)
+    units = hidden.shape[0]
+    across, down, corner = tp + 1 - 2 * (tp % 2), (tp + 2) % 4, 3 - tp
+    group = (across, down, corner)
     others = [(me + d) % count for d in range(1, count)]
     greet([(other, tp) for other in others] + [(me, other) for other in group])
 
@@ -378,14 +390,31 @@
             pl.ds(pl.multiple_of(owner * width, 128), width),
         ]
 
-    def share_copy(source, q):
+    order = others + [me]
+
+    def sides(step):
+        return (across, down) if step % 2 == 0 else (down, across)
+
+    def share_copy(step, q):
+        source, near = order[step], sides(step)[0]
         return remote(
-            share(source, group[q]),
+            share(source, corner if q == 1 else near),
             landed.at[q, source],
             send.at[source, q],
             recv.at[source, q],
             me,
-            group[q],
+            near,
+        )
+
+    def middle_copy(step):
+        source = order[step]
+        return remote(
+            middle.at[source],
+            landed.at[2, source],
+            send.at[source, 2],
+            recv.at[source, 2],
+            me,
+            sides(step)[1],
         )
 
     def back_copy(target):
@@ -398,23 +427,58 @@
             tp,
         )
 
-    order = others + [me]
-    for source in order:
-        for q in range(3):
-            share_copy(source, q).start()
-    gather = ChipGather(proj, proj_out, proj_sems, me, tp, count)
-    gather.start()
-    for step, source in enumerate(order):
+    def begin(step):
+        for q in (1, 0):
+            share_copy(step, q).start()
+
+    def forward(step):
+        source = order[step]
+        share_copy(step, 1).wait_recv()
+        own = share(source, sides(step)[1])[...].astype(jnp.float32)
+        middle[source] = (own + landed[1, source].astype(jnp.float32)).astype(jnp.bfloat16)
+        middle_copy(step).start()
+
+    def settle(step):
+        source = order[step]
+        share_copy(step, 0).wait_recv()
+        middle_copy(step).wait_recv()
         total = share(source, tp)[...].astype(jnp.float32)
-        for q in range(3):
-            share_copy(source, q).wait_recv()
-            total = total + landed[q, source].astype(jnp.float32)
-        total = total.astype(jnp.bfloat16)
+        total = total + landed[0, source].astype(jnp.float32)
+        total = (total + landed[2, source].astype(jnp.float32)).astype(jnp.bfloat16)
         if step < count - 1:
             reduced[source] = total
             back_copy(source).start()
         else:
             back[pl.ds(pl.multiple_of(me * capacity, capacity), capacity), :] = total
+
+    pieces = 4 if units % 64 == 0 else 1
+    tile = units // pieces
+    spots = pieces * 4
+    products = ((gate_delta, expert_in), (up_delta, expert_in), (hidden, expert_cot))
+
+    def product(spot, carry):
+        rows = pl.ds(pl.multiple_of(spot // 4 * tile, 16), tile)
+        columns = pl.ds(pl.multiple_of(spot % 4 * width, 128), width)
+        for a, (left, right) in enumerate(products):
+            value = jnp.dot(
+                left[rows, :], right[:, columns], preferred_element_type=jnp.float32
+            )
+            grads[a, rows, columns] = value.astype(jnp.bfloat16)
+        return carry
+
+    window = min(3, count)
+    for step in range(window):
+        begin(step)
+    gather = ChipGather(proj, proj_out, proj_sems, me, tp, count)
+    gather.start()
+    for step in range(count):
+        lax.fori_loop(spots * step // count, spots * (step + 1) // count, product, 0)
+        if step + window < count:
+            begin(step + window)
+        forward(step)
+        if step >= 1:
+            settle(step - 1)
+    settle(count - 1)
     gather.pass_on()
     for other in others:
         remote(
@@ -437,15 +501,16 @@
         wide_copy(q).start()
     for q in range(3):
         wide_copy(q).wait()
-    for source in order:
-        for q in range(3):
-            share_copy(source, q).wait_send()
+    for step in range(count):
+        share_copy(step, 0).wait_send()
+        share_copy(step, 1).wait_send()
+        middle_copy(step).wait_send()
     for other in others:
         back_copy(other).wait_send()
     gather.finish()
 
 
-def combine(partial_value, cot, pick, proj, count):
+def combine(partial_value, cot, pick, proj, hidden, gate_delta, up_delta, rows, rows_cot, count):
     tokens, width = cot.shape
     capacity = partial_value.shape[0] // count
     return pl.pallas_call(
@@ -453,11 +518,13 @@
         out_shape=(
             jax.ShapeDtypeStruct((tokens, partial_value.shape[1]), jnp.bfloat16),
             jax.ShapeDtypeStruct((count * proj.shape[0], proj.shape[1]), jnp.bfloat16),
-        ),
-        in_specs=[VMEM] * 4,
-        out_specs=(VMEM,) * 2,
+            jax.ShapeDtypeStruct((3, hidden.shape[0], partial_value.shape[1]), jnp.bfloat16),
+        ),
+        in_specs=[VMEM] * 9,
+        out_specs=(VMEM,) * 3,
         scratch_shapes=[
             pltpu.VMEM((3, count, capacity, width), jnp.bfloat16),
+            pltpu.VMEM((count, capacity, width), jnp.bfloat16),
             pltpu.VMEM((count, capacity, width), jnp.bfloat16),
             pltpu.VMEM((count * capacity, width), jnp.bfloat16),
             pltpu.SemaphoreType.DMA((count, 3)),
@@ -472,7 +539,12 @@
             collective_id=1, has_side_effects=True, vmem_limit_bytes=40 << 20
         ),
         name="combine",
-    )(partial_value, cot, pick, proj)
+        cost_estimate=pl.CostEstimate(
+            flops=6 * hidden.size * partial_value.shape[1],
+            bytes_accessed=50 * partial_value.size * 2,
+            transcendentals=0,
+        ),
+    )(partial_value, cot, pick, proj, hidden, gate_delta, up_delta, rows, rows_cot)
 
 
 def module_kernel(
@@ -528,7 +600,9 @@
     for other in others:
         strip_copy(other).start()
     mixed_grad = jnp.dot(stream[...], proj[...], preferred_element_type=jnp.float32)
-    normed = (conv_out[...].astype(jnp.float32) - row_mean[...]) * row_rstd[...]
+    rstd = jnp.broadcast_to(row_rstd[...], (tokens, tokens)).T[:, 0:1]
+    mean = jnp.broadcast_to(row_mean[...], (tokens, tokens)).T[:, 0:1]
+    normed = (conv_out[...].astype(jnp.float32) - mean) * rstd
     scaled = normed * gain[...]
     sig = jax.nn.sigmoid(scaled)
     norm_grad = mixed_grad * sig * (1.0 + scaled * (1.0 - sig)) * gain[...]
@@ -550,7 +624,7 @@
     total = sums[...] + arrived[0] + arrived[1] + arrived[2]
     total = total * (1.0 / (channels * 4))
     means = jnp.concatenate([total] * 16, axis=0).T
-    conv_grad = row_rstd[...] * (norm_grad - means[:, 0:1] - normed * means[:, 1:2])
+    conv_grad = rstd * (norm_grad - means[:, 0:1] - normed * means[:, 1:2])
     extended[:tokens] = conv_grad
     edge = remote(
         extended.at[pl.ds(0, halo)],
@@ -691,32 +765,36 @@
     gate_w = w_gate[0]
     up_w = w_up[0]
     down_w = w_down[0]
-    gate_pre = contract_cols(expert_in, gate_w)
-    up_pre = contract_cols(expert_in, up_w)
+    gate_pre = contract_cols(gate_w, expert_in)
+    up_pre = contract_cols(up_w, expert_in)
     gate_sig = jax.nn.sigmoid(gate_pre)
     gate_act = gate_pre * gate_sig
     hidden = (gate_act * up_pre).astype(jnp.bfloat16)
-    hidden_grad = contract_cols(expert_cot, down_w)
+    hidden_grad = contract_cols(down_w, expert_cot)
     gate_delta = (hidden_grad * up_pre * gate_sig * (1.0 + gate_pre * (1.0 - gate_sig))).astype(
         jnp.bfloat16
     )
     up_delta = (hidden_grad * gate_act).astype(jnp.bfloat16)
-    partial_value = jnp.dot(gate_delta, gate_w, preferred_element_type=jnp.float32) + jnp.dot(
-        up_delta, up_w, preferred_element_type=jnp.float32
-    )
-    stream_full, proj_full = combine(
-        partial_value.astype(jnp.bfloat16), cotangent, pick, out_proj, experts
-    )
-    down_g = contract_rows(hidden, expert_cot).astype(jnp.bfloat16)
-    gate_g = contract_rows(gate_delta, expert_in).astype(jnp.bfloat16)
-    up_g = contract_rows(up_delta, expert_in).astype(jnp.bfloat16)
+    partial_value = contract_rows(gate_delta, gate_w) + contract_rows(up_delta, up_w)
+    stream_full, proj_full, grads = combine(
+        partial_value.astype(jnp.bfloat16),
+        cotangent,
+        pick,
+        out_proj,
+        hidden,
+        gate_delta,
+        up_delta,
+        expert_in,
+        expert_cot,
+        experts,
+    )
     proj_g, value_g, gating_g = module(
         stream_full,
         proj_full,
         mixed_all,
         conv_out,
-        row_mean[:, None],
-        row_rstd[:, None],
+        row_mean[None, :],
+        row_rstd[None, :],
         ln_gain[None, :],
         taps,
         v_value,
@@ -724,7 +802,7 @@
         experts,
     )
     stream = lax.dynamic_slice_in_dim(stream_full, lax.axis_index("tp") * width, width, 1)
-    return (gate_g[None], up_g[None], down_g[None], proj_g, stream, value_g, gating_g)
+    return (grads[0:1], grads[1:2], grads[2:3], proj_g, stream, value_g, gating_g)
 
 
 def shards(*blocks):

time: 147 us -> 135 us (0.918)
  matrix products: 22.7 us -> 10.2 us
  Pallas kernels: 103 us -> 109 us
  local copies, waits for them, and re-layouts: 17.7 us -> 12.7 us
    unnamed x72 -> x34, local copies, waits for them, and re-layouts: 13.8 us -> 4.9 us
    dot_general x5 -> x4, matrix products: 13.1 us -> 4.38 us  [contract_rows(): lax.dot_general(left, right, (((0,), (0,)), ((), ())), preferred_element_...]
    slice x0 -> x1, local copies, waits for them, and re-layouts: none -> 6.07 us  [kernel_shards(): grads[2:3]]
    pallas_call x1, Pallas kernels: 43.4 us -> 49 us  [combine(): pl.pallas_call(functools.partial(combine_kernel, count), out_shape=(jax.S...]
    dot_general x2 -> x0, matrix products: 3.87 us -> none  [the longest x1 1.99 us: kernel_shards(): jnp.dot(up_delta, up_w, preferred_element_type=jnp.float32)]
    broadcast_in_dim x2 -> x0, local copies, waits for them, and re-layouts: 2.15 us -> none  [the longest x1 1.39 us: kernel_shards(): row_rstd[:, None]]
where the time goes in v2:
time: 135 us
  Pallas kernels  109 us (81%)
  local copies, waits for them, and re-layouts  12.7 us (9%)
  matrix products  10.2 us (8%)
  other arithmetic  2.22 us (2%)
    pallas_call x1, Pallas kernels, combine(): pl.pallas_call(functools.partial(combine_kernel, count), out_shape=(jax.S...  49 us
    pallas_call x1, Pallas kernels, dispatch(): pl.pallas_call(functools.partial(dispatch_kernel, count), out_shape=(full...  43 us
    pallas_call x1, Pallas kernels, module(): pl.pallas_call(functools.partial(module_kernel, count), out_shape=(jax.Sh...  17 us
    slice x1, local copies, waits for them, and re-layouts, kernel_shards(): grads[2:3]  6.07 us
    dot_general x3, matrix products, contract_cols(): lax.dot_general(left, right, (((1,), (1,)), ((), ())), preferred_element_...  5.59 us
    unnamed x34, local copies, waits for them, and re-layouts  4.9 us
    dot_general x4, matrix products, contract_rows(): lax.dot_general(left, right, (((0,), (0,)), ((), ())), preferred_element_...  4.38 us

profile of v2, /device:TPU:13, one launch (start us, length us, event | category | flops | bytes accessed | tf_op | source)
XLA Modules:
  0.0 135.1 jit_solution(9573087688970722427)
XLA Ops:
  0.7 0.9 copy.28
  1.6 0.1 eq.45
  1.8 0.2 fusion.19
  2.0 0.1 convert_element_type.56
  2.2 0.9 multiply_add_fusion
  3.2 0.8 slice_bitcast_fusion.1
  3.9 1.0 fusion.20
  5.0 0.3 convolution_convert_fusion
  5.3 0.4 convolution_convert_fusion.1
  5.7 0.1 multiply_convert_fusion.3.mixed
  5.9 43.0 %dispatch.1 = (bf16[512,2048]{1,0:T(8,128)(2,1)S(1)}, bf16[512,2048]{1,0:T(8,128)(2,1)S(1)}, bf16[1024,256]{1,0:T(8,128)(2,1)S(1)}) custom-call(bf16[8,64,512]{2,1,0:T(8,128)(2,1)S(1)} %bitcast.46, bf16[8,64,512]{2,1,0:T(8,128)(2,1)S(1)} %bitcast.47, bf16[128,256]{1,0:T(8,128)(2,1)S(1)} %multiply_convert_fusion.3.mixed), custom_call_target="tpu_custom_call" | custom-call | bytes 104857600 | tf_op jit(solution)/shard_map/dispatch/pallas_call | solution.py:328
  48.9 1.7 %fusion.15 = f32[704,512]{1,0:T(8,128)S(1)} fusion(bf16[512,2048]{1,0:T(8,128)(2,1)S(1)} %get-tuple-element.17.expert_in, bf16[1,704,2048]{2,1,0:T(8,128)(2,1)S(1)} %copy-done.12), kind=kOutput, calls=%fused_computation.12 | convolution fusion | flops 1476395008 | bytes 6422528 | tf_op jit(solution)/shard_map/dot_general | solution.py:34
  50.7 1.7 %fusion.9 = f32[704,512]{1,0:T(8,128)S(1)} fusion(bf16[512,2048]{1,0:T(8,128)(2,1)S(1)} %get-tuple-element.16.expert_cot, bf16[1,704,2048]{2,1,0:T(8,128)(2,1)S(1)} %copy-done.14), kind=kOutput, calls=%fused_computation.10 | convolution fusion | flops 1476395008 | bytes 6422528 | tf_op jit(solution)/shard_map/dot_general | solution.py:34
  52.4 2.2 %multiply_convert_fusion = (bf16[704,512]{1,0:T(8,128)(2,1)S(1)}, bf16[704,512]{1,0:T(8,128)(2,1)S(1)}, bf16[704,512]{1,0:T(8,128)(2,1)S(1)}) fusion(f32[704,512]{1,0:T(8,128)S(1)} %fusion.15, f32[704,512]{1,0:T(8,128)S(1)} %fusion.9, bf16[512,2048]{1,0:T(8,128)(2,1)S(1)} %get-tuple-element.17.expert_in, bf16[1,704,2048]{2,1,0:T(8,128)(2,1)S(1)} %copy-done), kind=kOutput, calls=%fused_computation.13 | convolution fusion | flops 1481801728 | bytes 10027008 | tf_op jit(solution)/shard_map/dot_general | solution.py:34
  54.7 1.8 %fusion = f32[512,2048]{1,0:T(8,128)S(1)} fusion(bf16[704,512]{1,0:T(8,128)(2,1)S(1)} %get-tuple-element.29.gate_delta, bf16[1,704,2048]{2,1,0:T(8,128)(2,1)S(1)} %copy-done.12), kind=kOutput, calls=%fused_computation.1 | convolution fusion | flops 1476395008 | bytes 7798784 | tf_op jit(solution)/shard_map/dot_general | solution.py:28
  56.5 1.8 %add_convert_fusion.partial_ref = bf16[512,2048]{1,0:T(8,128)(2,1)S(1)} fusion(f32[512,2048]{1,0:T(8,128)S(1)} %fusion, bf16[704,512]{1,0:T(8,128)(2,1)S(1)} %get-tuple-element.30.up_delta, bf16[1,704,2048]{2,1,0:T(8,128)(2,1)S(1)} %copy-done), kind=kOutput, calls=%fused_computation | convolution fusion | flops 1478492160 | bytes 9895936 | tf_op jit(solution)/shard_map/dot_general | solution.py:28
  58.4 0.1 fusion.30.pick
  58.5 49.0 %combine.1 = (bf16[128,2048]{1,0:T(8,128)(2,1)S(1)}, bf16[2048,256]{1,0:T(8,128)(2,1)S(1)}, bf16[3,704,2048]{2,1,0:T(8,128)(2,1)}) custom-call(bf16[512,2048]{1,0:T(8,128)(2,1)S(1)} %add_convert_fusion.partial_ref, bf16[128,512]{1,0:T(8,128)(2,1)S(1)} %copy-done.3, bf16[128,512]{1,0:T(8,128)(2,1)S(1)} %fusion.30.pick, bf16[256,256]{1,0:T(8,128)(2,1)S(1)} %copy-done.11, ...), custom_call_target="tpu_custom_call" | custom-call | flops 4429185024 | bytes 104857600 | tf_op jit(solution)/shard_map/combine/pallas_call | solution.py:516
  107.5 17.0 %module.1 = (f32[256,256]{1,0:T(8,128)S(1)}, bf16[128,256]{1,0:T(8,128)(2,1)S(1)}, bf16[128,256]{1,0:T(8,128)(2,1)S(1)}) custom-call(bf16[128,2048]{1,0:T(8,128)(2,1)S(1)} %get-tuple-element.19.stream, bf16[2048,256]{1,0:T(8,128)(2,1)S(1)} %get-tuple-element.20.proj, bf16[1024,256]{1,0:T(8,128)(2,1)S(1)} %get-tuple-element.21.mixed, ...), custom_call_target="tpu_custom_call" | custom-call | tf_op jit(solution)/shard_map/module/pallas_call | solution.py:681
  124.5 6.1 %fusion.35 = (bf16[1,704,2048]{2,1,0:T(8,128)(2,1)}, bf16[1,704,2048]{2,1,0:T(8,128)(2,1)}, bf16[1,704,2048]{2,1,0:T(8,128)(2,1)}) fusion(bf16[3,704,2048]{2,1,0:T(8,128)(2,1)} %get-tuple-element.18), kind=kLoop, calls=%fused_computation.49 | loop fusion | bytes 17301504 | tf_op jit(solution)/shard_map/slice | solution.py:805
  130.6 0.7 constant_dynamic-slice_fusion
  131.3 1.7 %copy.33 = f32[256,256]{1,0:T(8,128)} copy(f32[256,256]{1,0:T(8,128)} %copy-done.1) | data formatting | bytes 524288
  133.0 1.5 %copy.34 = bf16[128,256]{1,0:T(8,128)(2,1)} copy(bf16[128,256]{1,0:T(8,128)(2,1)} %copy-done.4) | data formatting | bytes 131072
  134.4 0.6 copy.35
  (34 shorter events, 0.4 us)
Async XLA Ops:
  0.6 51.8 %copy-start = (bf16[1,704,2048]{2,1,0:T(8,128)(2,1)S(1)}, bf16[1,704,2048]{2,1,0:T(8,128)(2,1)}, u32[]{:S(2)}) copy-start(bf16[1,704,2048]{2,1,0:T(8,128)(2,1)} %param.20) | copy-start | bytes 8650756
  0.6 4.6 %copy-start.13 = (bf16[128,512]{1,0:T(8,128)(2,1)S(1)}, bf16[128,512]{1,0:T(8,128)(2,1)}, u32[]{:S(2)}) copy-start(bf16[128,512]{1,0:T(8,128)(2,1)} %param.15) | copy-start | bytes 393220
  0.7 5.0 %copy-start.2 = (bf16[128,256]{1,0:T(8,128)(2,1)S(1)}, bf16[128,256]{1,0:T(8,128)(2,1)}, u32[]{:S(2)}) copy-start(bf16[128,256]{1,0:T(8,128)(2,1)} %conv_out.1) | copy-start | bytes 196612
  0.7 5.0 %copy-start.10 = (f32[128]{0:T(128)S(1)}, f32[128]{0:T(128)}, u32[]{:S(2)}) copy-start(f32[128]{0:T(128)} %param.25) | copy-start | bytes 1540
  0.7 5.0 %copy-start.9 = (f32[128]{0:T(128)S(1)}, f32[128]{0:T(128)}, u32[]{:S(2)}) copy-start(f32[128]{0:T(128)} %param.26) | copy-start | bytes 1540
  0.7 5.0 %copy-start.8 = (f32[256]{0:T(256)S(1)}, f32[256]{0:T(256)}, u32[]{:S(2)}) copy-start(f32[256]{0:T(256)} %param.27) | copy-start | bytes 3076
  2.2 46.7 %copy-start.12 = (bf16[1,704,2048]{2,1,0:T(8,128)(2,1)S(1)}, bf16[1,704,2048]{2,1,0:T(8,128)(2,1)}, u32[]{:S(2)}) copy-start(bf16[1,704,2048]{2,1,0:T(8,128)(2,1)} %param.19) | copy-start | bytes 8650756
  48.9 1.8 %copy-start.14 = (bf16[1,704,2048]{2,1,0:T(8,128)(2,1)S(1)}, bf16[1,704,2048]{2,1,0:T(8,128)(2,1)}, u32[]{:S(2)}) copy-start(bf16[1,704,2048]{2,1,0:T(8,128)(2,1)} %param.21) | copy-start | bytes 8650756
  56.5 2.0 %copy-start.3 = (bf16[128,512]{1,0:T(8,128)(2,1)S(1)}, bf16[128,512]{1,0:T(8,128)(2,1)}, u32[]{:S(2)}) copy-start(bf16[128,512]{1,0:T(8,128)(2,1)} %cot.1) | copy-start | bytes 393220
  56.5 2.0 %copy-start.11 = (bf16[256,256]{1,0:T(8,128)(2,1)S(1)}, bf16[256,256]{1,0:T(8,128)(2,1)}, u32[]{:S(2)}) copy-start(bf16[256,256]{1,0:T(8,128)(2,1)} %proj.1) | copy-start | bytes 393220
  58.5 49.0 %copy-start.5 = (bf16[128,256]{1,0:T(8,128)(2,1)S(1)}, bf16[128,256]{1,0:T(8,128)(2,1)}, u32[]{:S(2)}) copy-start(bf16[128,256]{1,0:T(8,128)(2,1)} %v_value.1) | copy-start | bytes 196612
  58.5 49.0 %copy-start.6 = (bf16[128,256]{1,0:T(8,128)(2,1)S(1)}, bf16[128,256]{1,0:T(8,128)(2,1)}, u32[]{:S(2)}) copy-start(bf16[128,256]{1,0:T(8,128)(2,1)} %v_gate.1) | copy-start | bytes 196612
  58.5 49.0 %copy-start.7 = (bf16[31,256]{1,0:T(8,128)(2,1)S(1)}, bf16[31,256]{1,0:T(8,128)(2,1)}, u32[]{:S(2)}) copy-start(bf16[31,256]{1,0:T(8,128)(2,1)} %taps.1) | copy-start | bytes 47620
  124.5 6.1 %copy-start.1 = (f32[256,256]{1,0:T(8,128)}, f32[256,256]{1,0:T(8,128)S(1)}, u32[]{:S(2)}) copy-start(f32[256,256]{1,0:T(8,128)S(1)} %get-tuple-element.49) | copy-start | bytes 786436
  124.5 6.1 %copy-start.4 = (bf16[128,256]{1,0:T(8,128)(2,1)}, bf16[128,256]{1,0:T(8,128)(2,1)S(1)}, u32[]{:S(2)}) copy-start(bf16[128,256]{1,0:T(8,128)(2,1)S(1)} %get-tuple-element.51) | copy-start | bytes 196612
